TPU v7x, 32 devices: a whole 2x2x4 slice. The times are simulated.
32 devices in a mesh: fs: 8 (over z, x), tp: 4 (over y, core).
Axes of the slice: x: 2, y: 2, z: 4, core: 2. Of those that a mesh axis runs over, the one named last changes fastest.
Arguments:
- tokens: bfloat16 [4096, 2048], P(('fs', 'tp')), may hold values from -6 to 6
- gate_weight: bfloat16 [5632, 2048], P('tp', 'fs'), may hold values from -0.125 to 0.125
- up_weight: bfloat16 [5632, 2048], P('tp', 'fs'), may hold values from -0.125 to 0.125
- down_weight: bfloat16 [5632, 2048], P('tp', 'fs'), may hold values from -0.078125 to 0.078125
- out_grad: bfloat16 [4096, 2048], P(('fs', 'tp')), may hold values from -6 to 6
Outputs:
- grad_tokens: bfloat16 [4096, 2048], P(('fs', 'tp'))
- grad_gate: float32 [5632, 2048], P('tp', 'fs')
- grad_up: float32 [5632, 2048], P('tp', 'fs')
- grad_down: float32 [5632, 2048], P('tp', 'fs')
- gate_rows: float32 [5632], P('tp')
- up_rows: float32 [5632], P('tp')
- down_rows: float32 [5632], P('tp')
All inputs are finite; a program needn't handle non-finite values.
Results may differ from a plain program's by a relative error of at most 0.014.
Values may be sent and summed in bfloat16 or wider, within the bound.
A program may use at most 128 MiB of HBM per device.

v0:
```python
import math
import jax
import jax.numpy as jnp
from jax import lax
from jax.sharding import PartitionSpec as P


def body(tokens, gate_weight, up_weight, down_weight, out_grad):
    inputs, cotangent = (
        lax.all_gather(tokens, "tp", axis=0, tiled=True),
        lax.all_gather(out_grad, "tp", axis=0, tiled=True),
    )
    w_gate, w_up, w_down = (
        lax.all_gather(gate_weight, "fs", axis=1, tiled=True),
        lax.all_gather(up_weight, "fs", axis=1, tiled=True),
        lax.all_gather(down_weight, "fs", axis=1, tiled=True),
    )
    inner = (((1,), (1,)), ((), ()))
    gate = lax.dot_general(inputs, w_gate, inner, preferred_element_type=jnp.float32)
    up = lax.dot_general(inputs, w_up, inner, preferred_element_type=jnp.float32)
    dhidden = lax.dot_general(cotangent, w_down, inner, preferred_element_type=jnp.float32)
    sig = jax.nn.sigmoid(gate)
    silu = gate * sig
    act = (silu * up).astype(jnp.bfloat16)
    dgate = (dhidden * up * sig * (1.0 + gate * (1.0 - sig))).astype(jnp.bfloat16)
    dup = (dhidden * silu).astype(jnp.bfloat16)
    term = jnp.dot(dgate, w_gate, preferred_element_type=jnp.float32)
    grad_tokens = lax.psum_scatter(
        (term + jnp.dot(dup, w_up, preferred_element_type=jnp.float32)).astype(jnp.bfloat16),
        "tp",
        scatter_dimension=0,
        tiled=True,
    )
    factor = 1.0 / math.sqrt(inputs.shape[0] * lax.axis_size("fs"))
    outer = (((0,), (0,)), ((), ()))
    width = gate_weight.shape[1] * lax.axis_size("fs")
    part_gate = lax.dot_general(dgate, inputs, outer, preferred_element_type=jnp.float32) * factor
    part_up = lax.dot_general(dup, inputs, outer, preferred_element_type=jnp.float32) * factor
    part_down = lax.dot_general(act, cotangent, outer, preferred_element_type=jnp.float32) * factor
    grad_gate, grad_up, grad_down = (
        lax.psum_scatter(
            part_gate.astype(jnp.bfloat16), "fs", scatter_dimension=1, tiled=True
        ).astype(jnp.float32),
        lax.psum_scatter(
            part_up.astype(jnp.bfloat16), "fs", scatter_dimension=1, tiled=True
        ).astype(jnp.float32),
        lax.psum_scatter(
            part_down.astype(jnp.bfloat16), "fs", scatter_dimension=1, tiled=True
        ).astype(jnp.float32),
    )
    sums = lax.psum(
        (
            jnp.sum(grad_gate * grad_gate, axis=1),
            jnp.sum(grad_up * grad_up, axis=1),
            jnp.sum(grad_down * grad_down, axis=1),
        ),
        "fs",
    )
    gate_rows, up_rows, down_rows = (sums[0] / width, sums[1] / width, sums[2] / width)
    return (grad_tokens, grad_gate, grad_up, grad_down, gate_rows, up_rows, down_rows)


def solution(mesh):
    return jax.shard_map(
        body,
        mesh=mesh,
        in_specs=(
            P(("fs", "tp"), None),
            P("tp", "fs"),
            P("tp", "fs"),
            P("tp", "fs"),
            P(("fs", "tp"), None),
        ),
        out_specs=(
            P(("fs", "tp"), None),
            P("tp", "fs"),
            P("tp", "fs"),
            P("tp", "fs"),
            P("tp"),
            P("tp"),
            P("tp"),
        ),
        check_vma=False,
    )
```

profile of v0, /device:TPU:0, one launch (start us, length us, event | category | flops | bytes accessed | tf_op | source)
XLA Modules:
  0.0 727.2 jit_solution(359217630501200977)
XLA Ops:
  7.2 0.7 all-gather.10.cloned.1.call-update
  7.9 0.7 all-gather.12.cloned.1.call-update
  8.7 0.7 all-gather.14.cloned.1.call-update
  10.6 24.3 %all-gather.10.cloned.1.call-done = bf16[512,2048]{1,0:T(8,128)(2,1)} async-done(((bf16[128,2048]{1,0:T(8,128)(2,1)}), bf16[512,2048]{1,0:T(8,128)(2,1)}) %all-gather.10.cloned.1.call-update) | async-done | bytes 2097168 | tf_op jit(solution)/shard_map/all_gather | solution.py:10
  34.9 95.2 %all-gather.12.cloned.1.call-done = bf16[1408,2048]{1,0:T(8,128)(2,1)} async-done(((bf16[1408,256]{1,0:T(8,128)(2,1)}), bf16[1408,2048]{1,0:T(8,128)(2,1)}) %all-gather.12.cloned.1.call-update) | async-done | bytes 5767184 | tf_op jit(solution)/shard_map/all_gather | solution.py:15
  130.1 8.3 %fusion.3 = f32[512,1408]{1,0:T(8,128)} fusion(bf16[512,2048]{1,0:T(8,128)(2,1)} %all-gather.10.cloned.1.call-done, bf16[1408,2048]{1,0:T(8,128)(2,1)} %all-gather.12.cloned.1.call-done), kind=kOutput, calls=%fused_computation.16 | convolution fusion | flops 2952790016 | bytes 10747904 | tf_op jit(solution)/shard_map/dot_general | solution.py:20
  138.4 85.1 %all-gather.14.cloned.1.call-done = bf16[1408,2048]{1,0:T(8,128)(2,1)} async-done(((bf16[1408,256]{1,0:T(8,128)(2,1)}), bf16[1408,2048]{1,0:T(8,128)(2,1)}) %all-gather.14.cloned.1.call-update) | async-done | bytes 5767184 | tf_op jit(solution)/shard_map/all_gather | solution.py:14
  223.5 7.6 %fusion.4 = f32[512,1408]{1,0:T(8,128)} fusion(bf16[512,2048]{1,0:T(8,128)(2,1)S(1)} %copy-done, bf16[1408,2048]{1,0:T(8,128)(2,1)} %all-gather.14.cloned.1.call-done), kind=kOutput, calls=%fused_computation.17 | convolution fusion | flops 2952790016 | bytes 10747904 | tf_op jit(solution)/shard_map/dot_general | solution.py:19
  231.1 14.6 %all-gather.6.cloned.1.call-done = bf16[512,2048]{1,0:T(8,128)(2,1)} async-done(((bf16[128,2048]{1,0:T(8,128)(2,1)}), bf16[512,2048]{1,0:T(8,128)(2,1)}) %all-gather.6.cloned.1.call-update) | async-done | bytes 2097168 | tf_op jit(solution)/shard_map/all_gather | solution.py:11
  245.7 9.1 %multiply_convert_fusion = bf16[1408,2048]{1,0:T(8,128)(2,1)} fusion(bf16[512,2048]{1,0:T(8,128)(2,1)} %all-gather.6.cloned.1.call-done, f32[512,1408]{1,0:T(8,128)} %fusion.3, f32[512,1408]{1,0:T(8,128)} %fusion.4), kind=kOutput, calls=%fused_computation | convolution fusion | flops 2962882560 | bytes 13631488 | tf_op jit(solution)/shard_map/dot_general | solution.py:39
  255.0 85.7 %all-gather.8.cloned.1.call-done = bf16[1408,2048]{1,0:T(8,128)(2,1)} async-done(((bf16[1408,256]{1,0:T(8,128)(2,1)}), bf16[1408,2048]{1,0:T(8,128)(2,1)}) %all-gather.8.cloned.1.call-update) | async-done | bytes 5767184 | tf_op jit(solution)/shard_map/all_gather | solution.py:16
  340.7 10.2 %multiply_convert_fusion.4 = (bf16[512,1408]{1,0:T(8,128)(2,1)S(1)}, bf16[512,1408]{1,0:T(8,128)(2,1)}) fusion(f32[512,1408]{1,0:T(8,128)} %fusion.4, f32[512,1408]{1,0:T(8,128)} %fusion.3, bf16[512,2048]{1,0:T(8,128)(2,1)} %all-gather.6.cloned.1.call-done, bf16[1408,2048]{1,0:T(8,128)(2,1)} %all-gather.8.cloned.1.call-done), kind=kOutput, calls=%fused_computation.5 | convolution fusion | flops 2962161664 | bytes 16515072 | tf_op jit(solution)/shard_map/dot_general | solution.py:21
  350.9 5.0 multiply_convert_fusion.1
  355.9 6.5 multiply_convert_fusion.2
  362.5 1.3 copy-done.1
  363.8 5.4 fusion.5
  369.2 7.4 %add_convert_fusion = bf16[512,2048]{1,0:T(8,128)(2,1)} fusion(f32[512,2048]{1,0:T(8,128)S(1)} %fusion.5, bf16[512,1408]{1,0:T(8,128)(2,1)S(1)} %get-tuple-element.16, bf16[1408,2048]{1,0:T(8,128)(2,1)} %all-gather.12.cloned.1.call-done), kind=kOutput, calls=%fused_computation.3 | convolution fusion | flops 2954887168 | bytes 13500416 | tf_op jit(solution)/shard_map/dot_general | solution.py:29
  376.6 76.8 %reduce-scatter.11.cloned.1.call-done = bf16[1408,256]{1,0:T(8,128)(2,1)} async-done(((bf16[1408,2048]{1,0:T(8,128)(2,1)}), bf16[1408,256]{1,0:T(8,128)(2,1)}) %reduce-scatter.11.cloned.1.call-update) | async-done | bytes 720912 | tf_op jit(solution)/shard_map/reduce_scatter | solution.py:47
  453.5 2.3 multiply_reduce_fusion
  455.8 111.8 %reduce-scatter.9.cloned.1.call-done = bf16[1408,256]{1,0:T(8,128)(2,1)} async-done(((bf16[1408,2048]{1,0:T(8,128)(2,1)}), bf16[1408,256]{1,0:T(8,128)(2,1)}) %reduce-scatter.9.cloned.1.call-update) | async-done | bytes 720912 | tf_op jit(solution)/shard_map/reduce_scatter | solution.py:44
  567.6 2.3 multiply_reduce_fusion.1
  569.9 111.8 %reduce-scatter.7.cloned.1.call-done = bf16[1408,256]{1,0:T(8,128)(2,1)} async-done(((bf16[1408,2048]{1,0:T(8,128)(2,1)}), bf16[1408,256]{1,0:T(8,128)(2,1)}) %reduce-scatter.7.cloned.1.call-update) | async-done | bytes 720912 | tf_op jit(solution)/shard_map/reduce_scatter | solution.py:41
  681.7 2.3 multiply_reduce_fusion.2
  684.0 35.5 %all-reduce = (f32[1408]{0:T(1024)S(1)}, f32[1408]{0:T(1024)S(1)}, f32[1408]{0:T(1024)S(1)}) all-reduce(f32[1408]{0:T(1024)S(1)} %get-tuple-element.14, f32[1408]{0:T(1024)S(1)} %get-tuple-element.12, f32[1408]{0:T(1024)S(1)} %get-tuple-element.10), channel_id=1, replica_groups=mesh['fs'=8,'tp'=4] {'fs'}, use_global_device_ids=true, to_apply=%region_5.0 | all-reduce | flops 4224 | bytes 33792 | tf_op jit(solution)/shard_map/psum | solution.py:51
  (21 shorter events, 2.9 us)
Async XLA Ops:
  7.2 27.7 %all-gather.10.cloned.1.call-start = ((), (), s32[]{:S(2)}) async-start(), calls=%async_computation.6 | async-start | bytes 2621440 | tf_op jit(solution)/shard_map/all_gather | solution.py:10
  7.9 122.2 %all-gather.12.cloned.1.call-start = ((), (), s32[]{:S(2)}) async-start(), calls=%async_computation.7 | async-start | bytes 6488064 | tf_op jit(solution)/shard_map/all_gather | solution.py:15
  8.6 214.8 %all-gather.14.cloned.1.call-start = ((), (), s32[]{:S(2)}) async-start(), calls=%async_computation.8 | async-start | bytes 6488064 | tf_op jit(solution)/shard_map/all_gather | solution.py:14
  9.4 236.3 %all-gather.6.cloned.1.call-start = ((), (), s32[]{:S(2)}) async-start(), calls=%async_computation.4 | async-start | bytes 2621440 | tf_op jit(solution)/shard_map/all_gather | solution.py:11
  10.0 330.7 %all-gather.8.cloned.1.call-start = ((), (), s32[]{:S(2)}) async-start(), calls=%async_computation.5 | async-start | bytes 6488064 | tf_op jit(solution)/shard_map/all_gather | solution.py:16
  10.5 442.9 %reduce-scatter.11.cloned.1.call-start = ((), (), s32[]{:S(2)}) async-start(), calls=%async_computation.12 | async-start | bytes 6488064 | tf_op jit(solution)/shard_map/reduce_scatter | solution.py:47
  34.9 188.6 %copy-start = (bf16[512,2048]{1,0:T(8,128)(2,1)S(1)}, bf16[512,2048]{1,0:T(8,128)(2,1)}, u32[]{:S(2)}) copy-start(bf16[512,2048]{1,0:T(8,128)(2,1)} %all-gather.10.cloned.1.call-done) | copy-start | bytes 6291460
  254.7 312.8 %reduce-scatter.9.cloned.1.call-start = ((), (), s32[]{:S(2)}) async-start(), calls=%async_computation.11 | async-start | bytes 6488064 | tf_op jit(solution)/shard_map/reduce_scatter | solution.py:44
  355.9 325.8 %reduce-scatter.7.cloned.1.call-start = ((), (), s32[]{:S(2)}) async-start(), calls=%async_computation.10 | async-start | bytes 6488064 | tf_op jit(solution)/shard_map/reduce_scatter | solution.py:41
  362.4 1.4 copy-start.1
  362.4 358.3 %reduce-scatter.5.cloned.1.call-start = ((), (), s32[]{:S(2)}) async-start(), calls=%async_computation.9 | async-start | bytes 2621440 | tf_op jit(solution)/shard_map/reduce_scatter | solution.py:28
Sparse Core Ops, SparseCore 0:
  9.5 25.2 all-gather.9
  36.9 93.1 all-gather.11
  132.1 91.3 all-gather.13
  224.9 20.7 all-gather.5
  247.5 93.1 all-gather.7
  344.2 109.1 reduce-scatter.10
  457.1 110.3 reduce-scatter.8
  571.2 110.3 reduce-scatter.6
  684.8 30.5 reduce-scatter.4
where the time goes:
time: 728 us; the launch traced here: 727 us
  waiting for transfers between devices  608 us (84%)
  matrix products  59.5 us (8%)
  blocking collectives  35.5 us (5%)
  between operations  13.9 us (2%)
  other arithmetic  8.24 us (1%)
    reduce_scatter x1, waiting for transfers between devices, body(): lax.psum_scatter(part_up.astype(jnp.bfloat16), 'fs', scatter_dimension=1,...  112 us
    reduce_scatter x1, waiting for transfers between devices, body(): lax.psum_scatter(part_gate.astype(jnp.bfloat16), 'fs', scatter_dimension=...  112 us
    all_gather x1, waiting for transfers between devices, body(): lax.all_gather(up_weight, 'fs', axis=1, tiled=True)  95.2 us
    all_gather x1, waiting for transfers between devices, body(): lax.all_gather(down_weight, 'fs', axis=1, tiled=True)  85.7 us
    all_gather x1, waiting for transfers between devices, body(): lax.all_gather(gate_weight, 'fs', axis=1, tiled=True)  85.1 us
    reduce_scatter x1, waiting for transfers between devices, body(): lax.psum_scatter(part_down.astype(jnp.bfloat16), 'fs', scatter_dimension=...  76.8 us
    psum x1, blocking collectives, body(): lax.psum((jnp.sum(grad_gate * grad_gate, axis=1), jnp.sum(grad_up * grad_...  35.5 us
    all_gather x1, waiting for transfers between devices, body(): lax.all_gather(tokens, 'tp', axis=0, tiled=True)  24.3 us
  transfers between devices with their start and end apart: 9, of which 8 were waited for; matrix products, arithmetic and copies ran while one was open for 9% of the time, Pallas kernels for 0%

commit v1 on v0

--- a/solution.py
+++ b/solution.py
@@ -5,15 +5,33 @@
 from jax.sharding import PartitionSpec as P
 
 
+def _trace_sheet(vector, join_dim):
+    d_next = list(vector.shape[1:])
+    d_next[join_dim] *= vector.shape[0]
+    return jnp.moveaxis(vector, 0, join_dim).reshape(d_next)
+
+
 def body(tokens, gate_weight, up_weight, down_weight, out_grad):
     inputs, cotangent = (
         lax.all_gather(tokens, "tp", axis=0, tiled=True),
         lax.all_gather(out_grad, "tp", axis=0, tiled=True),
     )
+
+    def fit_gates(inner_x, axis_tag, dim_i=1):
+        dev_n = lax.axis_size(axis_tag)
+        store = [inner_x]
+        crops = [(idx, (idx + 1) % dev_n) for idx in range(dev_n)]
+        while len(store) < dev_n:
+            store.append(lax.ppermute(store[-1], axis_tag, crops))
+        mat_out = lax.axis_index(axis_tag)
+        placed = jnp.stack(store, 0)
+        store = placed[(mat_out - jnp.arange(dev_n)) % dev_n]
+        return _trace_sheet(store, dim_i)
+
     w_gate, w_up, w_down = (
         lax.all_gather(gate_weight, "fs", axis=1, tiled=True),
         lax.all_gather(up_weight, "fs", axis=1, tiled=True),
-        lax.all_gather(down_weight, "fs", axis=1, tiled=True),
+        fit_gates(down_weight, "fs"),
     )
     inner = (((1,), (1,)), ((), ()))
     gate = lax.dot_general(inputs, w_gate, inner, preferred_element_type=jnp.float32)

time: 728 us -> 704 us (0.967)
  waiting for transfers between devices: 608 us -> 559 us
  local copies, waits for them, and re-layouts: 1.29 us -> 24.9 us
    ppermute x0 -> x7, waiting for transfers between devices: none -> 180 us  [fit_gates(): store.append(lax.ppermute(store[-1], axis_tag, crops))]
    all_gather x1, waiting for transfers between devices: 95.2 us -> 0.01 us  [body(): lax.all_gather(up_weight, 'fs', axis=1, tiled=True)]
    all_gather x1 -> x0, waiting for transfers between devices: 85.7 us -> none  [body(): lax.all_gather(down_weight, 'fs', axis=1, tiled=True)]
    reduce_scatter x1, waiting for transfers between devices: 76.8 us -> 112 us  [body(): lax.psum_scatter(part_down.astype(jnp.bfloat16), 'fs', scatter_dimension=...]
    reduce_scatter x1, waiting for transfers between devices: 112 us -> 80.6 us  [body(): lax.psum_scatter(part_up.astype(jnp.bfloat16), 'fs', scatter_dimension=1,...]
    all_gather x1, waiting for transfers between devices: 85.1 us -> 58.9 us  [body(): lax.all_gather(gate_weight, 'fs', axis=1, tiled=True)]
    all_gather x1, waiting for transfers between devices: 24.3 us -> 0.01 us  [body(): lax.all_gather(tokens, 'tp', axis=0, tiled=True)]
    unnamed x4 -> x15, local copies, waits for them, and re-layouts: 1.29 us -> 9.64 us
  transfers between devices with their start and end apart: 9 -> 15, of which waited for: 8 -> 12; matrix products, arithmetic and copies ran while one was open for 9% -> 10% of each run, Pallas kernels for 0% -> 0%
where the time goes in v1:
time: 704 us
  waiting for transfers between devices  559 us (79%)
  matrix products  58.2 us (8%)
  blocking collectives  35.5 us (5%)
  local copies, waits for them, and re-layouts  24.9 us (4%)
  between operations  14.2 us (2%)
  other arithmetic  8.26 us (1%)
    ppermute x7, waiting for transfers between devices, fit_gates(): store.append(lax.ppermute(store[-1], axis_tag, crops))  180 us
    reduce_scatter x1, waiting for transfers between devices, body(): lax.psum_scatter(part_down.astype(jnp.bfloat16), 'fs', scatter_dimension=...  112 us
    reduce_scatter x1, waiting for transfers between devices, body(): lax.psum_scatter(part_gate.astype(jnp.bfloat16), 'fs', scatter_dimension=...  112 us
    reduce_scatter x1, waiting for transfers between devices, body(): lax.psum_scatter(part_up.astype(jnp.bfloat16), 'fs', scatter_dimension=1,...  80.6 us
    all_gather x1, waiting for transfers between devices, body(): lax.all_gather(gate_weight, 'fs', axis=1, tiled=True)  58.9 us
    psum x1, blocking collectives, body(): lax.psum((jnp.sum(grad_gate * grad_gate, axis=1), jnp.sum(grad_up * grad_...  35.5 us
    all_gather x1, waiting for transfers between devices, body(): lax.all_gather(out_grad, 'tp', axis=0, tiled=True)  14.8 us
  transfers between devices with their start and end apart: 15, of which 12 were waited for; matrix products, arithmetic and copies ran while one was open for 10% of the time, Pallas kernels for 0%

profile of v1, /device:TPU:0, one launch (start us, length us, event | category | flops | bytes accessed | tf_op | source)
XLA Modules:
  0.0 703.8 jit_solution(16290445469296143164)
XLA Ops:
  9.4 3.0 collective-permute-start
  12.5 19.4 %collective-permute-done = bf16[1408,256]{1,0:T(8,128)(2,1)S(1)} collective-permute-done((bf16[1408,256]{1,0:T(8,128)(2,1)}, bf16[1408,256]{1,0:T(8,128)(2,1)S(1)}, u32[]{:S(2)}, u32[]{:S(2)}) %collective-permute-start) | collective-permute-done | bytes 720928 | tf_op jit(solution)/shard_map/ppermute | solution.py:25
  31.8 21.9 %collective-permute-done.1 = bf16[1408,256]{1,0:T(8,128)(2,1)S(1)} collective-permute-done((bf16[1408,256]{1,0:T(8,128)(2,1)S(1)}, bf16[1408,256]{1,0:T(8,128)(2,1)S(1)}, u32[]{:S(2)}, u32[]{:S(2)}) %collective-permute-start.1) | collective-permute-done | bytes 720928 | tf_op jit(solution)/shard_map/ppermute | solution.py:25
  53.8 32.9 %collective-permute-done.2 = bf16[1408,256]{1,0:T(8,128)(2,1)S(1)} collective-permute-done((bf16[1408,256]{1,0:T(8,128)(2,1)S(1)}, bf16[1408,256]{1,0:T(8,128)(2,1)S(1)}, u32[]{:S(2)}, u32[]{:S(2)}) %collective-permute-start.2) | collective-permute-done | bytes 720928 | tf_op jit(solution)/shard_map/ppermute | solution.py:25
  87.7 24.3 %collective-permute-done.3 = bf16[1408,256]{1,0:T(8,128)(2,1)S(1)} collective-permute-done((bf16[1408,256]{1,0:T(8,128)(2,1)S(1)}, bf16[1408,256]{1,0:T(8,128)(2,1)S(1)}, u32[]{:S(2)}, u32[]{:S(2)}) %collective-permute-start.3) | collective-permute-done | bytes 720928 | tf_op jit(solution)/shard_map/ppermute | solution.py:25
  114.0 33.5 %collective-permute-done.4 = bf16[1408,256]{1,0:T(8,128)(2,1)S(1)} collective-permute-done((bf16[1408,256]{1,0:T(8,128)(2,1)S(1)}, bf16[1408,256]{1,0:T(8,128)(2,1)S(1)}, u32[]{:S(2)}, u32[]{:S(2)}) %collective-permute-start.4) | collective-permute-done | bytes 720928 | tf_op jit(solution)/shard_map/ppermute | solution.py:25
  149.2 33.5 %collective-permute-done.5 = bf16[1408,256]{1,0:T(8,128)(2,1)S(1)} collective-permute-done((bf16[1408,256]{1,0:T(8,128)(2,1)S(1)}, bf16[1408,256]{1,0:T(8,128)(2,1)S(1)}, u32[]{:S(2)}, u32[]{:S(2)}) %collective-permute-start.5) | collective-permute-done | bytes 720928 | tf_op jit(solution)/shard_map/ppermute | solution.py:25
  184.6 14.1 %collective-permute-done.6 = bf16[1408,256]{1,0:T(8,128)(2,1)S(1)} collective-permute-done((bf16[1408,256]{1,0:T(8,128)(2,1)S(1)}, bf16[1408,256]{1,0:T(8,128)(2,1)S(1)}, u32[]{:S(2)}, u32[]{:S(2)}) %collective-permute-start.6) | collective-permute-done | bytes 720928 | tf_op jit(solution)/shard_map/ppermute | solution.py:25
  199.7 6.1 gather_fusion
  205.7 8.3 %copy.22 = bf16[1408,8,256]{0,2,1:T(8,128)(2,1)} copy(bf16[1408,8,256]{2,0,1:T(8,128)(2,1)} %bitcast.37) | data formatting | bytes 11534336 | tf_op jit(solution)/shard_map/transpose | solution.py:11
  214.0 8.2 %fusion.5 = f32[512,1408]{0,1:T(8,128)} fusion(bf16[512,2048]{1,0:T(8,128)(2,1)} %all-gather.7.cloned.1.call-done, bf16[1408,2048]{1,0:T(8,128)(2,1)} %all-gather.9.cloned.1.call-done), kind=kOutput, calls=%fused_computation.33 | convolution fusion | flops 2952790016 | bytes 10747904 | tf_op jit(solution)/shard_map/dot_general | solution.py:38
  222.2 58.9 %all-gather.11.cloned.1.call-done = bf16[1408,2048]{1,0:T(8,128)(2,1)} async-done(((bf16[1408,256]{1,0:T(8,128)(2,1)}), bf16[1408,2048]{1,0:T(8,128)(2,1)}) %all-gather.11.cloned.1.call-update) | async-done | bytes 5767184 | tf_op jit(solution)/shard_map/all_gather | solution.py:32
  281.1 7.4 %fusion.6 = f32[512,1408]{0,1:T(8,128)} fusion(bf16[512,2048]{1,0:T(8,128)(2,1)S(1)} %copy-done.1, bf16[1408,2048]{1,0:T(8,128)(2,1)} %all-gather.11.cloned.1.call-done), kind=kOutput, calls=%fused_computation.34 | convolution fusion | flops 2952790016 | bytes 10747904 | tf_op jit(solution)/shard_map/dot_general | solution.py:37
  288.5 14.8 %all-gather.5.cloned.1.call-done = bf16[512,2048]{1,0:T(8,128)(2,1)} async-done(((bf16[128,2048]{1,0:T(8,128)(2,1)}), bf16[512,2048]{1,0:T(8,128)(2,1)}) %all-gather.5.cloned.1.call-update) | async-done | bytes 2097168 | tf_op jit(solution)/shard_map/all_gather | solution.py:17
  303.3 10.4 %multiply_convert_fusion.4 = (bf16[512,1408]{0,1:T(8,128)(2,1)S(1)}, bf16[512,1408]{0,1:T(8,128)(2,1)}) fusion(f32[512,1408]{0,1:T(8,128)} %fusion.6, f32[512,1408]{0,1:T(8,128)} %fusion.5, bf16[1408,2048]{0,1:T(8,128)(2,1)} %bitcast.38, bf16[512,2048]{1,0:T(8,128)(2,1)} %all-gather.5.cloned.1.call-done), kind=kOutput, calls=%fused_computation.7 | convolution fusion | flops 2962161664 | bytes 16515072 | tf_op jit(solution)/shard_map/dot_general | solution.py:39
  313.7 5.0 multiply_convert_fusion.1
  318.8 6.5 multiply_convert_fusion.2
  327.3 7.9 %multiply_convert_fusion = bf16[1408,2048]{1,0:T(8,128)(2,1)} fusion(bf16[512,2048]{1,0:T(8,128)(2,1)S(1)} %copy-done.2, f32[512,1408]{0,1:T(8,128)} %fusion.5, f32[512,1408]{0,1:T(8,128)} %fusion.6), kind=kOutput, calls=%fused_computation.1 | convolution fusion | flops 2962882560 | bytes 13631488 | tf_op jit(solution)/shard_map/dot_general | solution.py:57
  336.5 5.5 fusion.7
  342.0 7.4 %add_convert_fusion = bf16[512,2048]{1,0:T(8,128)(2,1)} fusion(f32[512,2048]{1,0:T(8,128)S(1)} %fusion.7, bf16[512,1408]{0,1:T(8,128)(2,1)S(1)} %get-tuple-element.16, bf16[1408,2048]{1,0:T(8,128)(2,1)} %all-gather.9.cloned.1.call-done), kind=kOutput, calls=%fused_computation.4 | convolution fusion | flops 2954887168 | bytes 13500416 | tf_op jit(solution)/shard_map/dot_general | solution.py:47
  349.4 80.6 %reduce-scatter.9.cloned.1.call-done = bf16[1408,256]{1,0:T(8,128)(2,1)} async-done(((bf16[1408,2048]{1,0:T(8,128)(2,1)}), bf16[1408,256]{1,0:T(8,128)(2,1)}) %reduce-scatter.9.cloned.1.call-update) | async-done | bytes 720912 | tf_op jit(solution)/shard_map/reduce_scatter | solution.py:62
  432.3 111.6 %reduce-scatter.7.cloned.1.call-done = bf16[1408,256]{1,0:T(8,128)(2,1)} async-done(((bf16[1408,2048]{1,0:T(8,128)(2,1)}), bf16[1408,256]{1,0:T(8,128)(2,1)}) %reduce-scatter.7.cloned.1.call-update) | async-done | bytes 720912 | tf_op jit(solution)/shard_map/reduce_scatter | solution.py:59
  546.2 111.7 %reduce-scatter.11.cloned.1.call-done = bf16[1408,256]{1,0:T(8,128)(2,1)} async-done(((bf16[1408,2048]{1,0:T(8,128)(2,1)}), bf16[1408,256]{1,0:T(8,128)(2,1)}) %reduce-scatter.11.cloned.1.call-update) | async-done | bytes 720912 | tf_op jit(solution)/shard_map/reduce_scatter | solution.py:65
  660.2 35.5 %all-reduce = (f32[1408]{0:T(1024)S(1)}, f32[1408]{0:T(1024)S(1)}, f32[1408]{0:T(1024)S(1)}) all-reduce(f32[1408]{0:T(1024)S(1)} %get-tuple-element.14, f32[1408]{0:T(1024)S(1)} %get-tuple-element.12, f32[1408]{0:T(1024)S(1)} %get-tuple-element.10), channel_id=1, replica_groups=mesh['fs'=8,'tp'=4] {'fs'}, use_global_device_ids=true, to_apply=%region_5.6 | all-reduce | flops 4224 | bytes 33792 | tf_op jit(solution)/shard_map/psum | solution.py:69
  (48 shorter events, 21.3 us)
Async XLA Ops:
  7.2 79.6 %copy-start = (bf16[1408,256]{1,0:T(8,128)(2,1)S(1)}, bf16[1408,256]{1,0:T(8,128)(2,1)}, u32[]{:S(2)}) copy-start(bf16[1408,256]{1,0:T(8,128)(2,1)} %param.8) | copy-start | bytes 2162692
  7.2 206.8 %all-gather.7.cloned.1.call-start = ((), (), s32[]{:S(2)}) async-start(), calls=%async_computation.5 | async-start | bytes 2621440 | tf_op jit(solution)/shard_map/all_gather | solution.py:16
  7.9 206.1 %all-gather.9.cloned.1.call-start = ((), (), s32[]{:S(2)}) async-start(), calls=%async_computation.6 | async-start | bytes 6488064 | tf_op jit(solution)/shard_map/all_gather | solution.py:33
  8.7 272.4 %all-gather.11.cloned.1.call-start = ((), (), s32[]{:S(2)}) async-start(), calls=%async_computation.7 | async-start | bytes 6488064 | tf_op jit(solution)/shard_map/all_gather | solution.py:32
  9.4 293.9 %all-gather.5.cloned.1.call-start = ((), (), s32[]{:S(2)}) async-start(), calls=%async_computation.4 | async-start | bytes 2621440 | tf_op jit(solution)/shard_map/all_gather | solution.py:17
  9.4 22.4 %collective-permute-start = (bf16[1408,256]{1,0:T(8,128)(2,1)}, bf16[1408,256]{1,0:T(8,128)(2,1)S(1)}, u32[]{:S(2)}, u32[]{:S(2)}) collective-permute-start(bf16[1408,256]{1,0:T(8,128)(2,1)} %param.8), channel_id=1, source_target_pairs={{0,4},{4,8},{8,12},{12,16},{16,20},{20,24},{24,28},{28,0},{1,5},{5... | collective-permute-start | bytes 2162696 | tf_op jit(solution)/shard_map/ppermute | solution.py:25
  31.8 21.9 %collective-permute-start.1 = (bf16[1408,256]{1,0:T(8,128)(2,1)S(1)}, bf16[1408,256]{1,0:T(8,128)(2,1)S(1)}, u32[]{:S(2)}, u32[]{:S(2)}) collective-permute-start(bf16[1408,256]{1,0:T(8,128)(2,1)S(1)} %collective-permute-done), channel_id=1, source_target_pairs={{0,4},{4,8},{8,12},{12,16},{16,20},{20,24},{24,28},{28,0},{1,5},{5... | collective-permute-start | bytes 2162696 | tf_op jit(solution)/shard_map/ppermute | solution.py:25
  53.8 33.0 %collective-permute-start.2 = (bf16[1408,256]{1,0:T(8,128)(2,1)S(1)}, bf16[1408,256]{1,0:T(8,128)(2,1)S(1)}, u32[]{:S(2)}, u32[]{:S(2)}) collective-permute-start(bf16[1408,256]{1,0:T(8,128)(2,1)S(1)} %collective-permute-done.1), channel_id=1, source_target_pairs={{0,4},{4,8},{8,12},{12,16},{16,20},{20,24},{24,28},{28,0},{1,5},{5... | collective-permute-start | bytes 2162696 | tf_op jit(solution)/shard_map/ppermute | solution.py:25
  53.8 376.2 %reduce-scatter.9.cloned.1.call-start = ((), (), s32[]{:S(2)}) async-start(), calls=%async_computation.10 | async-start | bytes 6488064 | tf_op jit(solution)/shard_map/reduce_scatter | solution.py:62
  86.8 25.3 %collective-permute-start.3 = (bf16[1408,256]{1,0:T(8,128)(2,1)S(1)}, bf16[1408,256]{1,0:T(8,128)(2,1)S(1)}, u32[]{:S(2)}, u32[]{:S(2)}) collective-permute-start(bf16[1408,256]{1,0:T(8,128)(2,1)S(1)} %collective-permute-done.2), channel_id=1, source_target_pairs={{0,4},{4,8},{8,12},{12,16},{16,20},{20,24},{24,28},{28,0},{1,5},{5... | collective-permute-start | bytes 2162696 | tf_op jit(solution)/shard_map/ppermute | solution.py:25
  112.1 35.4 %collective-permute-start.4 = (bf16[1408,256]{1,0:T(8,128)(2,1)S(1)}, bf16[1408,256]{1,0:T(8,128)(2,1)S(1)}, u32[]{:S(2)}, u32[]{:S(2)}) collective-permute-start(bf16[1408,256]{1,0:T(8,128)(2,1)S(1)} %collective-permute-done.3), channel_id=1, source_target_pairs={{0,4},{4,8},{8,12},{12,16},{16,20},{20,24},{24,28},{28,0},{1,5},{5... | collective-permute-start | bytes 2162696 | tf_op jit(solution)/shard_map/ppermute | solution.py:25
  147.4 35.4 %collective-permute-start.5 = (bf16[1408,256]{1,0:T(8,128)(2,1)S(1)}, bf16[1408,256]{1,0:T(8,128)(2,1)S(1)}, u32[]{:S(2)}, u32[]{:S(2)}) collective-permute-start(bf16[1408,256]{1,0:T(8,128)(2,1)S(1)} %collective-permute-done.4), channel_id=1, source_target_pairs={{0,4},{4,8},{8,12},{12,16},{16,20},{20,24},{24,28},{28,0},{1,5},{5... | collective-permute-start | bytes 2162696 | tf_op jit(solution)/shard_map/ppermute | solution.py:25
  182.8 15.9 %collective-permute-start.6 = (bf16[1408,256]{1,0:T(8,128)(2,1)S(1)}, bf16[1408,256]{1,0:T(8,128)(2,1)S(1)}, u32[]{:S(2)}, u32[]{:S(2)}) collective-permute-start(bf16[1408,256]{1,0:T(8,128)(2,1)S(1)} %collective-permute-done.5), channel_id=1, source_target_pairs={{0,4},{4,8},{8,12},{12,16},{16,20},{20,24},{24,28},{28,0},{1,5},{5... | collective-permute-start | bytes 2162696 | tf_op jit(solution)/shard_map/ppermute | solution.py:25
  214.0 67.1 %copy-start.1 = (bf16[512,2048]{1,0:T(8,128)(2,1)S(1)}, bf16[512,2048]{1,0:T(8,128)(2,1)}, u32[]{:S(2)}) copy-start(bf16[512,2048]{1,0:T(8,128)(2,1)} %all-gather.7.cloned.1.call-done) | copy-start | bytes 6291460
  318.7 225.1 %reduce-scatter.7.cloned.1.call-start = ((), (), s32[]{:S(2)}) async-start(), calls=%async_computation.9 | async-start | bytes 6488064 | tf_op jit(solution)/shard_map/reduce_scatter | solution.py:59
  325.3 2.0 copy-start.2
  325.3 332.6 %reduce-scatter.11.cloned.1.call-start = ((), (), s32[]{:S(2)}) async-start(), calls=%async_computation.11 | async-start | bytes 6488064 | tf_op jit(solution)/shard_map/reduce_scatter | solution.py:65
  335.2 1.4 copy-start.3
  335.2 361.7 %reduce-scatter.5.cloned.1.call-start = ((), (), s32[]{:S(2)}) async-start(), calls=%async_computation.8 | async-start | bytes 2621440 | tf_op jit(solution)/shard_map/reduce_scatter | solution.py:46
Sparse Core Ops, SparseCore 0:
  9.5 25.2 all-gather.6
  36.9 137.1 all-gather.8
  176.1 104.9 all-gather.10
  282.5 20.7 all-gather.4
  318.9 111.0 reduce-scatter.8
  433.5 110.3 reduce-scatter.6
  547.5 110.3 reduce-scatter.10
  661.0 30.4 reduce-scatter.4
